TPU v7x, 32 devices: a whole 2x2x4 slice. The times are simulated.
32 devices in a mesh: sp: 8 (over z, y), tp: 4 (over x, core).
Axes of the slice: x: 2, y: 2, z: 4, core: 2. Of those that a mesh axis runs over, the one named last changes fastest.
Arguments:
- prompt_input: bfloat16 [2304, 2048], P('sp'), may hold values from -6 to 6
- next_input: bfloat16 [2048], replicated, may hold values from -6 to 6
- norm_gain: float32 [2048], replicated, may hold values from 0.1 to 1.9
- w_key: bfloat16 [2048, 1024], P(None, 'tp'), may hold values from -0.125 to 0.125
- w_value: bfloat16 [2048, 1024], P(None, 'tp'), may hold values from -0.125 to 0.125
- w_query: bfloat16 [2048, 1024], P(None, 'tp'), may hold values from -0.125 to 0.125
- key_offset: float32 [2304, 8], P('sp', 'tp'), may hold values from -10 to 0, as said below
Outputs:
- key_cache: bfloat16 [8, 8, 36, 1024], P('sp', None, None, 'tp')
- value_cache: bfloat16 [8, 8, 36, 1024], P('sp', None, None, 'tp')
- reading: bfloat16 [1024], replicated
Inputs may be any that keep to these rules, and one draw needn't show every extreme that they name: `key_offset`: finite log-odds offsets, one per key and head.
All inputs are finite; a program needn't handle non-finite values.
Results may differ from a plain program's by a relative error of at most 0.011.
Values may be sent and summed in bfloat16 or wider, within the bound.
A program may use at most 64 MiB of HBM per device.

v0:
```python
import functools

import jax
import jax.numpy as jnp
from jax import lax
from jax.experimental import pallas as pl
from jax.experimental.pallas import tpu as pltpu
from jax.sharding import PartitionSpec as P

HEAD_DIM = 128
MESH = pl.DeviceIdType.MESH


def norm_rows(rows, gain):
    wide = rows.astype(jnp.float32)
    inv_rms = lax.rsqrt(jnp.mean(wide * wide, axis=-1, keepdims=True) + 1e-06)
    return (wide * inv_rms * gain).astype(jnp.bfloat16)


def split_parts(wide, count):
    parts = []
    for _ in range(count):
        part = wide.astype(jnp.bfloat16).astype(jnp.float32)
        parts.append(part)
        wide = wide - part
    return jnp.concatenate(parts, axis=0).astype(jnp.bfloat16)


def fold_parts(rows, heads):
    total = rows[:heads]
    for first in range(heads, rows.shape[0], heads):
        total = total + rows[first : first + heads]
    return total


def kernel(
    n_sp, n_tp, chunks,
    x_hbm, next_hbm, gain_hbm, wk_hbm, wv_hbm, wq_hbm, offset_hbm,
    landed, read_out,
    x_in, normed, next_in, gain_in, wk, wv, wq, offset,
    outgoing, message, gathered, head_message, head_gathered,
    x_sem, load_sem, own_sem,
    b_ssem, b_rsem, m_ssem, m_rsem, h_ssem, h_rsem,
):
    me = lax.axis_index("sp")
    lane = lax.axis_index("tp")
    span, width = x_hbm.shape[0], wk_hbm.shape[1]
    heads = width // HEAD_DIM
    sub = span // n_sp
    rows = span // chunks

    load_gain, load_next, load_offset, load_key, load_query, load_value = [
        pltpu.make_async_copy(hbm, vmem, load_sem.at[n])
        for n, (hbm, vmem) in enumerate(
            [
                (gain_hbm, gain_in),
                (next_hbm, next_in),
                (offset_hbm, offset),
                (wk_hbm, wk),
                (wq_hbm, wq),
                (wv_hbm, wv),
            ]
        )
    ]
    x_loads = [
        pltpu.make_async_copy(
            x_hbm.at[pl.ds(c * rows, rows)], x_in.at[pl.ds(c * rows, rows)], x_sem.at[c]
        )
        for c in range(chunks)
    ]
    load_gain.start()
    for load in x_loads:
        load.start()
    load_key.start()
    load_next.start()
    load_offset.start()

    barrier = pltpu.get_barrier_semaphore()

    @pl.loop(1, n_sp)
    def _(step):
        pl.semaphore_signal(
            barrier, inc=1, device_id=(lax.rem(me + step, n_sp), lane), device_id_type=MESH
        )

    @pl.loop(1, n_tp)
    def _(step):
        pl.semaphore_signal(
            barrier, inc=1, device_id=(me, lax.rem(lane + step, n_tp)), device_id_type=MESH
        )

    load_gain.wait()
    gain = gain_in[...]
    step_rows = 16 if rows % 16 == 0 else rows
    for c in range(chunks):
        x_loads[c].wait()
        if c == 0:
            load_query.start()
        if c == chunks - 1:
            load_value.start()
        for first in range(c * rows, (c + 1) * rows, step_rows):
            normed[first : first + step_rows, :] = norm_rows(x_in[first : first + step_rows, :], gain)

    load_key.wait()
    wide_keys = jnp.dot(normed[...], wk[...], preferred_element_type=jnp.float32)
    keys = wide_keys.astype(jnp.bfloat16)

    load_next.wait()
    load_offset.wait()
    load_query.wait()
    next_row = next_in[...].astype(jnp.float32)
    next_row = jnp.concatenate([next_row[n : n + 1] for n in range(next_row.shape[0])], axis=1)
    query_normed = jnp.broadcast_to(norm_rows(next_row, gain), (16, x_hbm.shape[1]))
    query = jnp.dot(query_normed, wq[...], preferred_element_type=jnp.float32)
    row_ids = lax.broadcasted_iota(jnp.int32, query.shape, 0)
    head_ids = lax.broadcasted_iota(jnp.int32, query.shape, 1) // HEAD_DIM
    query = jnp.where(row_ids == head_ids, query, 0.0).astype(jnp.bfloat16)

    load_value.wait()
    logits = lax.dot_general(
        query, keys, (((1,), (1,)), ((), ())), preferred_element_type=jnp.float32
    )[:heads]
    logits = logits * HEAD_DIM ** (-0.5) + offset[...]
    tail = jnp.log1p(jnp.exp(-jnp.abs(logits)))
    log_breaks = -jnp.maximum(logits, 0.0) - tail
    later_than = (
        lax.broadcasted_iota(jnp.int32, (span, span), 0)
        > lax.broadcasted_iota(jnp.int32, (span, span), 1)
    )
    later_than = jnp.where(later_than, 1.0, 0.0).astype(jnp.bfloat16)
    inner = fold_parts(
        jnp.dot(split_parts(log_breaks, 3), later_than, preferred_element_type=jnp.float32), heads
    )
    block_total = jnp.sum(log_breaks, axis=1, keepdims=True)
    weights = jnp.exp(jnp.minimum(logits, 0.0) - tail + inner)

    wide_values = jnp.dot(normed[...], wv[...], preferred_element_type=jnp.float32)
    read = fold_parts(
        jnp.dot(
            split_parts(weights, 2),
            wide_values.astype(jnp.bfloat16),
            preferred_element_type=jnp.float32,
        ),
        heads,
    )
    for head in range(heads):
        message[head : head + 1, :] = read[head : head + 1, head * HEAD_DIM : (head + 1) * HEAD_DIM]
        message[heads + head : heads + head + 1, :] = jnp.broadcast_to(
            block_total[head : head + 1], (1, HEAD_DIM)
        )
    pl.semaphore_wait(barrier, n_sp + n_tp - 2)

    upper = me // ((n_sp + 1) // 2)

    def message_copy(step):
        return pltpu.make_async_remote_copy(
            src_ref=message, dst_ref=gathered.at[me],
            send_sem=m_ssem.at[step], recv_sem=m_rsem.at[step],
            device_id=(lax.rem(me + step, n_sp), lane), device_id_type=MESH,
        )

    def block_copy(step):
        to = lax.rem(me + step, n_sp)
        return pltpu.make_async_remote_copy(
            src_ref=outgoing.at[to], dst_ref=landed.at[me],
            send_sem=b_ssem.at[step], recv_sem=b_rsem.at[step],
            device_id=(to, lane), device_id_type=MESH,
        )

    @pl.loop(1, n_sp, unroll=n_sp <= 16)
    def _(near):
        message_copy(n_sp - near - upper * (n_sp - 2 * near)).start()

    for slot in range(n_sp):
        outgoing[slot] = jnp.concatenate(
            [
                wide[slot * sub : (slot + 1) * sub, head * HEAD_DIM : (head + 1) * HEAD_DIM]
                for wide in (wide_keys, wide_values)
                for head in range(heads)
            ],
            axis=0,
        ).astype(jnp.bfloat16)

    @pl.loop(1, n_sp)
    def _(near):
        block_copy(n_sp - near - upper * (n_sp - 2 * near)).start()

    own_message = pltpu.make_async_copy(message, gathered.at[me], own_sem.at[0])
    own_message.start()
    own_block = pltpu.make_async_copy(outgoing.at[me], landed.at[me], own_sem.at[1])
    own_block.start()
    own_message.wait()

    @pl.loop(1, n_sp)
    def _(step):
        message_copy(step).wait_recv()

    def add_block(step, carry):
        total, carried = carry
        block = gathered[n_sp - 1 - step]
        total = total + jnp.exp(carried) * block[:heads]
        return total, carried + block[heads : 2 * heads]

    zero = jnp.zeros((heads, HEAD_DIM), jnp.float32)
    total, _ = lax.fori_loop(0, n_sp, add_block, (zero, zero), unroll=n_sp <= 16)
    head_message[...] = total

    def head_copy(step):
        return pltpu.make_async_remote_copy(
            src_ref=head_message, dst_ref=head_gathered.at[lane],
            send_sem=h_ssem.at[step], recv_sem=h_rsem.at[step],
            device_id=(me, lax.rem(lane + step, n_tp)), device_id_type=MESH,
        )

    @pl.loop(1, n_tp, unroll=True)
    def _(step):
        head_copy(step).start()

    own_head = pltpu.make_async_copy(head_message, head_gathered.at[lane], own_sem.at[2])
    own_head.start()
    own_head.wait()

    @pl.loop(1, n_tp)
    def _(step):
        head_copy(step).wait_recv()

    read_out[...] = jnp.concatenate(
        [head_gathered[part] for part in range(n_tp)], axis=0
    ).astype(jnp.bfloat16)

    own_block.wait()

    @pl.loop(1, n_tp)
    def _(step):
        head_copy(step).wait_send()

    @pl.loop(1, n_sp)
    def _(step):
        message_copy(step).wait_send()
        block_copy(step).wait()


def finish(landed, read_in, k_out, v_out, read_out):
    sub, _, width = k_out.shape
    heads = width // HEAD_DIM
    for n, out in enumerate((k_out, v_out)):
        for head in range(heads):
            first = (n * heads + head) * sub
            piece = landed[...].astype(jnp.float32)[:, first : first + sub, :]
            out[:, :, head * HEAD_DIM : (head + 1) * HEAD_DIM] = jnp.swapaxes(
                piece, 0, 1
            ).astype(jnp.bfloat16)
    read_out[...] = read_in[...]


def shards(prompt_input, next_input, norm_gain, w_key, w_value, w_query, key_offset):
    span, depth = prompt_input.shape
    width = w_key.shape[1]
    heads = width // HEAD_DIM
    n_sp, n_tp = lax.axis_size("sp"), lax.axis_size("tp")
    sub = span // n_sp
    chunks = 3 if span % 48 == 0 else 1
    wide, narrow = jnp.float32, jnp.bfloat16
    blocks = (n_sp, 2 * heads * sub, HEAD_DIM)
    sems = pltpu.SemaphoreType.DMA
    landed = pl.pallas_call(
        functools.partial(kernel, n_sp, n_tp, chunks),
        out_shape=(
            jax.ShapeDtypeStruct(blocks, narrow),
            jax.ShapeDtypeStruct((n_tp * heads, HEAD_DIM), narrow),
        ),
        in_specs=[pl.BlockSpec(memory_space=pltpu.HBM)] * 7,
        out_specs=(pl.BlockSpec(memory_space=pltpu.VMEM),) * 2,
        scratch_shapes=[
            pltpu.VMEM((span, depth), narrow),
            pltpu.VMEM((span, depth), narrow),
            pltpu.VMEM((depth // HEAD_DIM, HEAD_DIM), narrow),
            pltpu.VMEM((1, depth), wide),
            pltpu.VMEM((depth, width), narrow),
            pltpu.VMEM((depth, width), narrow),
            pltpu.VMEM((depth, width), narrow),
            pltpu.VMEM((heads, span), wide),
            pltpu.VMEM(blocks, narrow),
            pltpu.VMEM((2 * heads, HEAD_DIM), wide),
            pltpu.VMEM((n_sp, 2 * heads, HEAD_DIM), wide),
            pltpu.VMEM((heads, HEAD_DIM), wide),
            pltpu.VMEM((n_tp, heads, HEAD_DIM), wide),
            sems((chunks,)),
            sems((6,)),
            sems((3,)),
            sems((n_sp,)),
            sems((n_sp,)),
            sems((n_sp,)),
            sems((n_sp,)),
            sems((n_tp,)),
            sems((n_tp,)),
        ],
        compiler_params=pltpu.CompilerParams(
            collective_id=0, has_side_effects=True, vmem_limit_bytes=16 * 2**20
        ),
        name="prefill",
    )(
        *[
            pltpu.with_memory_space_constraint(operand, pltpu.HBM)
            for operand in (
                prompt_input,
                next_input.reshape(-1, HEAD_DIM),
                norm_gain[None],
                w_key,
                w_value,
                w_query,
                key_offset.T,
            )
        ]
    )
    slotted = jax.ShapeDtypeStruct((sub, n_sp, width), narrow)
    key_cache, value_cache, reading = pl.pallas_call(
        finish,
        out_shape=(slotted, slotted, jax.ShapeDtypeStruct((n_tp * heads, HEAD_DIM), narrow)),
        in_specs=[pl.BlockSpec(memory_space=pltpu.VMEM)] * 2,
        out_specs=(pl.BlockSpec(memory_space=pltpu.VMEM),) * 3,
        compiler_params=pltpu.CompilerParams(vmem_limit_bytes=16 * 2**20),
        name="finish",
    )(*landed)
    return (
        jnp.swapaxes(key_cache, 0, 1)[None],
        jnp.swapaxes(value_cache, 0, 1)[None],
        reading.reshape(-1),
    )


def solution(mesh):
    placed = (P("sp", None), P(), P(), P(None, "tp"), P(None, "tp"), P(None, "tp"), P("sp", "tp"))
    return jax.shard_map(
        shards,
        mesh=mesh,
        in_specs=placed,
        out_specs=(P("sp", None, None, "tp"), P("sp", None, None, "tp"), P()),
        check_vma=False,
    )
```

profile of v0, /device:TPU:0, one launch (start us, length us, event | category | flops | bytes accessed | tf_op | source)
XLA Modules:
  0.0 16.7 jit_solution(15342544415194230661)
XLA Ops:
  0.6 15.3 %prefill.1 = (bf16[8,144,128]{2,1,0:T(8,128)(2,1)S(1)}, bf16[8,128]{1,0:T(8,128)(2,1)S(1)}) custom-call(bf16[288,2048]{1,0:T(8,128)(2,1)} %x_hbm.1, bf16[16,128]{1,0:T(8,128)(2,1)} %bitcast.11, f32[1,2048]{1,0:T(1,128)} %bitcast.10, bf16[2048,256]{1,0:T(8,128)(2,1)} %wk_hbm.1, bf16[2048,256]{1,0:T(8,128)(2,1)} %wv_hbm.1, bf16[2048,256]{1,0:T(8,128)(2,1)} %wq_hbm.1, ...), custom_call_target="tpu_custom_call" | custom-call | tf_op jit(solution)/shard_map/prefill/pallas_call | solution.py:266
  15.9 0.8 %finish.1 = (bf16[36,8,256]{2,1,0:T(8,128)(2,1)}, bf16[36,8,256]{2,1,0:T(8,128)(2,1)}, bf16[8,128]{1,0:T(8,128)(2,1)}) custom-call(bf16[8,144,128]{2,1,0:T(8,128)(2,1)S(1)} %get-tuple-element.8.landed, bf16[8,128]{1,0:T(8,128)(2,1)S(1)} %get-tuple-element.9.read_in), custom_call_target="tpu_custom_call" | custom-call | tf_op jit(solution)/shard_map/finish/pallas_call | solution.py:317
where the time goes:
time: 17 us; the launch traced here: 16.7 us
  Pallas kernels  16.1 us (95%)
  between operations  0.64 us (4%)
    pallas_call x1, Pallas kernels, shards(): pl.pallas_call(functools.partial(kernel, n_sp, n_tp, chunks), out_shape=(...  15.3 us
    pallas_call x1, Pallas kernels, shards(): pl.pallas_call(finish, out_shape=(slotted, slotted, jax.ShapeDtypeStruct(...  0.83 us

commit v1 on v0

v1 whole, which is shorter than its diff:
```python
import functools

import jax
import jax.numpy as jnp
from jax import lax
from jax.experimental import pallas as pl
from jax.experimental.pallas import tpu as pltpu
from jax.sharding import PartitionSpec as P

HEAD_DIM = 128
MESH = pl.DeviceIdType.MESH


def inverse_rms(wide):
    return lax.rsqrt(jnp.mean(wide * wide, axis=-1, keepdims=True) + 1e-06)


def split_parts(wide, count):
    parts = []
    for _ in range(count):
        part = wide.astype(jnp.bfloat16).astype(jnp.float32)
        parts.append(part)
        wide = wide - part
    return jnp.concatenate(parts, axis=0).astype(jnp.bfloat16)


def fold_parts(rows, heads):
    total = rows[:heads]
    for first in range(heads, rows.shape[0], heads):
        total = total + rows[first : first + heads]
    return total


def pack_blocks(wide, outgoing, landed, me, heads, sub):
    for slot in range(outgoing.shape[0]):
        outgoing[slot] = jnp.concatenate(
            [
                wide[slot * sub : (slot + 1) * sub, head * HEAD_DIM : (head + 1) * HEAD_DIM]
                for head in range(heads)
            ],
            axis=0,
        ).astype(jnp.bfloat16)
    landed[me] = outgoing[me]


def kernel(
    n_sp, n_tp, chunks,
    x_hbm, next_hbm, gain_hbm, wk_hbm, wv_hbm, wq_hbm, offset_hbm,
    k_landed, v_landed, read_out,
    x_in, scaled, inverse, next_in, gain_in, wk, wv, wq, offset, later_than,
    k_outgoing, v_outgoing, message, gathered,
    x_sem, load_sem,
    k_ssem, k_rsem, v_ssem, v_rsem, m_ssem, m_rsem, ready,
):
    me = lax.axis_index("sp")
    lane = lax.axis_index("tp")
    span, width = x_hbm.shape[0], wk_hbm.shape[1]
    heads = width // HEAD_DIM
    sub = span // n_sp
    rows = span // chunks
    unroll = n_sp <= 16

    load_gain, load_next, load_offset, load_key, load_query, load_value = [
        pltpu.make_async_copy(hbm, vmem, load_sem.at[n])
        for n, (hbm, vmem) in enumerate(
            [
                (gain_hbm, gain_in),
                (next_hbm, next_in),
                (offset_hbm, offset),
                (wk_hbm, wk),
                (wq_hbm, wq),
                (wv_hbm, wv),
            ]
        )
    ]
    x_loads = [
        pltpu.make_async_copy(
            x_hbm.at[pl.ds(c * rows, rows)], x_in.at[pl.ds(c * rows, rows)], x_sem.at[c]
        )
        for c in range(chunks)
    ]
    load_gain.start()
    for load in x_loads:
        load.start()
    load_key.start()
    load_next.start()
    load_offset.start()
    load_query.start()
    load_value.start()

    barrier = pltpu.get_barrier_semaphore()

    @pl.loop(1, n_sp)
    def _(step):
        pl.semaphore_signal(
            barrier, inc=1, device_id=(lax.rem(me + step, n_sp), lane), device_id_type=MESH
        )

    @pl.loop(1, n_tp)
    def _(step):
        pl.semaphore_signal(
            barrier, inc=1, device_id=(me, lax.rem(lane + step, n_tp)), device_id_type=MESH
        )

    later_than[...] = jnp.where(
        lax.broadcasted_iota(jnp.int32, (span, span), 0)
        > lax.broadcasted_iota(jnp.int32, (span, span), 1),
        1.0,
        0.0,
    ).astype(jnp.bfloat16)

    load_gain.wait()
    gain = gain_in[...]
    step_rows = 16 if rows % 16 == 0 else rows
    for c in range(chunks):
        x_loads[c].wait()
        for first in range(c * rows, (c + 1) * rows, step_rows):
            wide = x_in[first : first + step_rows, :].astype(jnp.float32)
            scaled[first : first + step_rows, :] = (wide * gain).astype(jnp.bfloat16)
            inverse[first : first + step_rows, :] = jnp.broadcast_to(
                inverse_rms(wide), (step_rows, HEAD_DIM)
            )

    def project(weight):
        wide = jnp.dot(scaled[...], weight[...], preferred_element_type=jnp.float32)
        factor = inverse[...]
        return jnp.concatenate(
            [
                wide[:, head * HEAD_DIM : (head + 1) * HEAD_DIM] * factor
                for head in range(heads)
            ],
            axis=1,
        )

    group = 2 if n_sp % 2 == 0 else 1
    groups = n_sp // group
    mine, place = me // group, lax.rem(me, group)
    upper = mine // ((groups + 1) // 2)

    def partner(order):
        near = order // group
        low = near + jnp.where(near >= mine, 1, 0)
        high = groups - 1 - near
        high = high - jnp.where(high <= mine, 1, 0)
        away = low * upper + high * (1 - upper)
        other = jnp.where(near >= groups - 1, 1, 0)
        chosen = away + other * (mine - away)
        return chosen * group + lax.rem(place + lax.rem(order, group) + other, group)

    def block_copy(outgoing, landed, ssem, rsem, order):
        to = partner(order)
        return pltpu.make_async_remote_copy(
            src_ref=outgoing.at[to], dst_ref=landed.at[me],
            send_sem=ssem.at[order], recv_sem=rsem.at[me],
            device_id=(to, lane), device_id_type=MESH,
        )

    def block_arrival(outgoing, landed, ssem, rsem, step):
        source = lax.rem(me + step, n_sp)
        return pltpu.make_async_remote_copy(
            src_ref=outgoing.at[source], dst_ref=landed.at[source],
            send_sem=ssem.at[step - 1], recv_sem=rsem.at[source],
            device_id=(source, lane), device_id_type=MESH,
        )

    keys_path = (k_outgoing, k_landed, k_ssem, k_rsem)
    values_path = (v_outgoing, v_landed, v_ssem, v_rsem)
    first_sends = group if n_sp > group else 0

    load_key.wait()
    wide_keys = project(wk)
    keys = wide_keys.astype(jnp.bfloat16)
    pack_blocks(wide_keys, k_outgoing, k_landed, me, heads, sub)

    pl.semaphore_wait(barrier, n_sp + n_tp - 2)
    for order in range(first_sends):
        block_copy(*keys_path, order).start()

    @pl.loop(1, n_tp)
    def _(step):
        pl.semaphore_signal(
            ready, inc=1, device_id=(me, lax.rem(lane + step, n_tp)), device_id_type=MESH
        )

    load_value.wait()
    wide_values = project(wv)
    pack_blocks(wide_values, v_outgoing, v_landed, me, heads, sub)
    for order in range(first_sends):
        block_copy(*values_path, order).start()

    load_next.wait()
    load_offset.wait()
    load_query.wait()
    next_row = next_in[...].astype(jnp.float32)
    next_row = jnp.concatenate([next_row[n : n + 1] for n in range(next_row.shape[0])], axis=1)
    next_scaled = jnp.broadcast_to((next_row * gain).astype(jnp.bfloat16), (16, x_hbm.shape[1]))
    query = jnp.dot(next_scaled, wq[...], preferred_element_type=jnp.float32)
    query = query * inverse_rms(next_row)
    row_ids = lax.broadcasted_iota(jnp.int32, query.shape, 0)
    head_ids = lax.broadcasted_iota(jnp.int32, query.shape, 1) // HEAD_DIM
    query = jnp.where(row_ids == head_ids, query, 0.0).astype(jnp.bfloat16)

    logits = lax.dot_general(
        query, keys, (((1,), (1,)), ((), ())), preferred_element_type=jnp.float32
    )[:heads]
    logits = logits * HEAD_DIM ** (-0.5) + offset[...]
    tail = jnp.log1p(jnp.exp(-jnp.abs(logits)))
    log_breaks = -jnp.maximum(logits, 0.0) - tail
    inner = fold_parts(
        jnp.dot(split_parts(log_breaks, 3), later_than[...], preferred_element_type=jnp.float32),
        heads,
    )
    block_total = jnp.sum(log_breaks, axis=1, keepdims=True)
    weights = jnp.exp(jnp.minimum(logits, 0.0) - tail + inner)
    read = fold_parts(
        jnp.dot(
            split_parts(weights, 2),
            wide_values.astype(jnp.bfloat16),
            preferred_element_type=jnp.float32,
        ),
        heads,
    )
    high = block_total.astype(jnp.bfloat16).astype(jnp.float32)
    low = block_total - high
    half = lax.broadcasted_iota(jnp.int32, (heads, HEAD_DIM), 1) < HEAD_DIM // 2
    message[...] = jnp.concatenate(
        [
            read[head : head + 1, head * HEAD_DIM : (head + 1) * HEAD_DIM]
            for head in range(heads)
        ]
        + [jnp.where(half, high, low)],
        axis=0,
    ).astype(jnp.bfloat16)
    gathered[me, lane] = message[...]

    pl.semaphore_wait(ready, n_tp - 1)

    def message_copy(order, step):
        to, to_lane = partner(order), lax.rem(lane + step, n_tp)
        return pltpu.make_async_remote_copy(
            src_ref=message, dst_ref=gathered.at[me, lane],
            send_sem=m_ssem.at[order, step], recv_sem=m_rsem.at[me, lane],
            device_id=(to, to_lane), device_id_type=MESH,
        )

    def own_message_copy(step):
        return pltpu.make_async_remote_copy(
            src_ref=message, dst_ref=gathered.at[me, lane],
            send_sem=m_ssem.at[n_sp - 1, step], recv_sem=m_rsem.at[me, lane],
            device_id=(me, lax.rem(lane + step, n_tp)), device_id_type=MESH,
        )

    def message_arrival(source, step):
        source_lane = lax.rem(lane + step, n_tp)
        return pltpu.make_async_remote_copy(
            src_ref=message, dst_ref=gathered.at[source, source_lane],
            send_sem=m_ssem.at[0, 0], recv_sem=m_rsem.at[source, source_lane],
            device_id=(source, source_lane), device_id_type=MESH,
        )

    @pl.loop(0, n_sp - 1, unroll=unroll)
    def _(order):
        for step in range(n_tp):
            message_copy(order, step).start()

    for step in range(1, n_tp):
        own_message_copy(step).start()

    @pl.loop(first_sends, n_sp - 1, unroll=unroll)
    def _(order):
        block_copy(*keys_path, order).start()
        block_copy(*values_path, order).start()

    for step in range(1, n_tp):
        message_arrival(me, step).wait_recv()

    @pl.loop(1, n_sp)
    def _(step):
        source = lax.rem(me + step, n_sp)
        for lane_step in range(n_tp):
            message_arrival(source, lane_step).wait_recv()

    def add_block(step, carry):
        block = [gathered[n_sp - 1 - step, part].astype(jnp.float32) for part in range(n_tp)]
        fresh = []
        for (total, carried), piece in zip(carry, block):
            total = total + jnp.exp(carried) * piece[:heads]
            halves = piece[heads:]
            fresh.append((total, carried + halves + pltpu.roll(halves, HEAD_DIM // 2, 1)))
        return tuple(fresh)

    zero = jnp.zeros((heads, HEAD_DIM), jnp.float32)
    totals = lax.fori_loop(0, n_sp, add_block, ((zero, zero),) * n_tp, unroll=unroll)
    read_out[...] = jnp.concatenate([total for total, _ in totals], axis=0).astype(jnp.bfloat16)

    for step in range(1, n_tp):
        own_message_copy(step).wait_send()

    @pl.loop(0, n_sp - 1)
    def _(order):
        for step in range(n_tp):
            message_copy(order, step).wait_send()
        block_copy(*keys_path, order).wait_send()
        block_copy(*values_path, order).wait_send()

    @pl.loop(1, n_sp)
    def _(step):
        block_arrival(*keys_path, step).wait_recv()
        block_arrival(*values_path, step).wait_recv()


def finish(k_landed, v_landed, read_in, k_out, v_out, read_out):
    sub, _, width = k_out.shape
    heads = width // HEAD_DIM
    for landed, out in ((k_landed, k_out), (v_landed, v_out)):
        for head in range(heads):
            piece = landed[...].astype(jnp.float32)[:, head * sub : (head + 1) * sub, :]
            out[:, :, head * HEAD_DIM : (head + 1) * HEAD_DIM] = jnp.swapaxes(
                piece, 0, 1
            ).astype(jnp.bfloat16)
    read_out[...] = read_in[...]


def shards(prompt_input, next_input, norm_gain, w_key, w_value, w_query, key_offset):
    span, depth = prompt_input.shape
    width = w_key.shape[1]
    heads = width // HEAD_DIM
    n_sp, n_tp = lax.axis_size("sp"), lax.axis_size("tp")
    sub = span // n_sp
    chunks = 3 if span % 48 == 0 else 1
    wide, narrow = jnp.float32, jnp.bfloat16
    blocks = (n_sp, heads * sub, HEAD_DIM)
    sems = pltpu.SemaphoreType.DMA
    landed = pl.pallas_call(
        functools.partial(kernel, n_sp, n_tp, chunks),
        out_shape=(
            jax.ShapeDtypeStruct(blocks, narrow),
            jax.ShapeDtypeStruct(blocks, narrow),
            jax.ShapeDtypeStruct((n_tp * heads, HEAD_DIM), narrow),
        ),
        in_specs=[pl.BlockSpec(memory_space=pltpu.HBM)] * 7,
        out_specs=(pl.BlockSpec(memory_space=pltpu.VMEM),) * 3,
        scratch_shapes=[
            pltpu.VMEM((span, depth), narrow),
            pltpu.VMEM((span, depth), narrow),
            pltpu.VMEM((span, HEAD_DIM), wide),
            pltpu.VMEM((depth // HEAD_DIM, HEAD_DIM), narrow),
            pltpu.VMEM((1, depth), wide),
            pltpu.VMEM((depth, width), narrow),
            pltpu.VMEM((depth, width), narrow),
            pltpu.VMEM((depth, width), narrow),
            pltpu.VMEM((heads, span), wide),
            pltpu.VMEM((span, span), narrow),
            pltpu.VMEM(blocks, narrow),
            pltpu.VMEM(blocks, narrow),
            pltpu.VMEM((2 * heads, HEAD_DIM), narrow),
            pltpu.VMEM((n_sp, n_tp, 2 * heads, HEAD_DIM), narrow),
            sems((chunks,)),
            sems((6,)),
            sems((n_sp,)),
            sems((n_sp,)),
            sems((n_sp,)),
            sems((n_sp,)),
            sems((n_sp, n_tp)),
            sems((n_sp, n_tp)),
            pltpu.SemaphoreType.REGULAR,
        ],
        compiler_params=pltpu.CompilerParams(
            collective_id=0, has_side_effects=True, vmem_limit_bytes=16 * 2**20
        ),
        name="prefill",
    )(
        *[
            pltpu.with_memory_space_constraint(operand, pltpu.HBM)
            for operand in (
                prompt_input,
                next_input.reshape(-1, HEAD_DIM),
                norm_gain[None],
                w_key,
                w_value,
                w_query,
                key_offset.T,
            )
        ]
    )
    slotted = jax.ShapeDtypeStruct((sub, n_sp, width), narrow)
    key_cache, value_cache, reading = pl.pallas_call(
        finish,
        out_shape=(slotted, slotted, jax.ShapeDtypeStruct((n_tp * heads, HEAD_DIM), narrow)),
        in_specs=[pl.BlockSpec(memory_space=pltpu.VMEM)] * 3,
        out_specs=(pl.BlockSpec(memory_space=pltpu.VMEM),) * 3,
        compiler_params=pltpu.CompilerParams(vmem_limit_bytes=16 * 2**20),
        name="finish",
    )(*landed)
    return (
        jnp.swapaxes(key_cache, 0, 1)[None],
        jnp.swapaxes(value_cache, 0, 1)[None],
        reading.reshape(-1),
    )


def solution(mesh):
    placed = (P("sp", None), P(), P(), P(None, "tp"), P(None, "tp"), P(None, "tp"), P("sp", "tp"))
    return jax.shard_map(
        shards,
        mesh=mesh,
        in_specs=placed,
        out_specs=(P("sp", None, None, "tp"), P("sp", None, None, "tp"), P()),
        check_vma=False,
    )
```

time: 17 us -> 18.5 us (1.088)
  Pallas kernels: 16.1 us -> 17.7 us
    pallas_call x1, Pallas kernels: 15.3 us -> 16.8 us  [shards(): pl.pallas_call(functools.partial(kernel, n_sp, n_tp, chunks), out_shape=(...]
where the time goes in v1:
time: 18.5 us; the launch traced here: 18.3 us
  Pallas kernels  17.7 us (96%)
  between operations  0.64 us (3%)
    pallas_call x1, Pallas kernels, shards(): pl.pallas_call(functools.partial(kernel, n_sp, n_tp, chunks), out_shape=(...  16.8 us
    pallas_call x1, Pallas kernels, shards(): pl.pallas_call(finish, out_shape=(slotted, slotted, jax.ShapeDtypeStruct(...  0.83 us

profile of v1, /device:TPU:0, one launch (start us, length us, event | category | flops | bytes accessed | tf_op | source)
XLA Modules:
  0.0 18.3 jit_solution(9959626113932774752)
XLA Ops:
  0.6 16.8 %prefill.1 = (bf16[8,72,128]{2,1,0:T(8,128)(2,1)S(1)}, bf16[8,72,128]{2,1,0:T(8,128)(2,1)S(1)}, bf16[8,128]{1,0:T(8,128)(2,1)S(1)}) custom-call(bf16[288,2048]{1,0:T(8,128)(2,1)} %x_hbm.1, bf16[16,128]{1,0:T(8,128)(2,1)} %bitcast.11, f32[1,2048]{1,0:T(1,128)} %bitcast.10, bf16[2048,256]{1,0:T(8,128)(2,1)} %wk_hbm.1, bf16[2048,256]{1,0:T(8,128)(2,1)} %wv_hbm.1, ...), custom_call_target="tpu_custom_call" | custom-call | tf_op jit(solution)/shard_map/prefill/pallas_call | solution.py:334
  17.5 0.8 %finish.1 = (bf16[36,8,256]{2,1,0:T(8,128)(2,1)}, bf16[36,8,256]{2,1,0:T(8,128)(2,1)}, bf16[8,128]{1,0:T(8,128)(2,1)}) custom-call(bf16[8,72,128]{2,1,0:T(8,128)(2,1)S(1)} %get-tuple-element.9.k_landed, bf16[8,72,128]{2,1,0:T(8,128)(2,1)S(1)} %get-tuple-element.10.v_landed, bf16[8,128]{1,0:T(8,128)(2,1)S(1)} %get-tuple-element.11.read_in), custom_call_target="tpu_custom_call" | custom-call | tf_op jit(solution)/shard_map/finish/pallas_call | solution.py:387

commit v2 on v1

v2 whole, which is shorter than its diff:
```python
import functools

import jax
import jax.numpy as jnp
from jax import lax
from jax.experimental import pallas as pl
from jax.experimental.pallas import tpu as pltpu
from jax.sharding import PartitionSpec as P

HEAD_DIM = 128
MESH = pl.DeviceIdType.MESH


def inverse_rms(wide):
    return lax.rsqrt(jnp.mean(wide * wide, axis=-1, keepdims=True) + 1e-06)


def split_parts(wide, count):
    parts = []
    for _ in range(count):
        part = wide.astype(jnp.bfloat16).astype(jnp.float32)
        parts.append(part)
        wide = wide - part
    return jnp.concatenate(parts, axis=0).astype(jnp.bfloat16)


def fold_parts(rows, heads):
    total = rows[:heads]
    for first in range(heads, rows.shape[0], heads):
        total = total + rows[first : first + heads]
    return total


def pack_blocks(wide, outgoing, first, heads, sub):
    for slot in range(wide.shape[0] // sub):
        outgoing[first + slot] = jnp.concatenate(
            [
                wide[slot * sub : (slot + 1) * sub, head * HEAD_DIM : (head + 1) * HEAD_DIM]
                for head in range(heads)
            ],
            axis=0,
        ).astype(jnp.bfloat16)


def kernel(
    n_sp, n_tp, chunks,
    x_hbm, next_hbm, gain_hbm, wk_hbm, wv_hbm, wq_hbm, offset_hbm,
    landed, read_out,
    x_in, scaled, keys, inverse, next_in, gain_in, wk, wv, wq, offset, later_than,
    outgoing, message, gathered,
    x_sem, load_sem,
    b_ssem, b_rsem, m_ssem, m_rsem, ready,
):
    me = lax.axis_index("sp")
    lane = lax.axis_index("tp")
    span, width = x_hbm.shape[0], wk_hbm.shape[1]
    heads = width // HEAD_DIM
    sub = span // n_sp
    rows = span // chunks
    unroll = n_sp <= 16

    upper = me // ((n_sp + 1) // 2)
    early = min(2, n_sp - 1)

    load_gain, load_next, load_offset, load_key, load_query, load_value = [
        pltpu.make_async_copy(hbm, vmem, load_sem.at[n])
        for n, (hbm, vmem) in enumerate(
            [
                (gain_hbm, gain_in),
                (next_hbm, next_in),
                (offset_hbm, offset),
                (wk_hbm, wk),
                (wq_hbm, wq),
                (wv_hbm, wv),
            ]
        )
    ]
    starts = [c * rows for c in range(chunks)]
    x_loads = [
        pltpu.make_async_copy(
            x_hbm.at[pl.ds(starts[c], rows)], x_in.at[pl.ds(starts[c], rows)], x_sem.at[c]
        )
        for c in range(chunks)
    ]
    load_gain.start()
    for load in x_loads:
        load.start()
    load_key.start()
    load_next.start()
    load_offset.start()

    barrier = pltpu.get_barrier_semaphore()

    @pl.loop(1, n_sp)
    def _(step):
        pl.semaphore_signal(
            barrier, inc=1, device_id=(lax.rem(me + step, n_sp), lane), device_id_type=MESH
        )

    @pl.loop(1, n_tp)
    def _(step):
        pl.semaphore_signal(
            barrier, inc=1, device_id=(me, lax.rem(lane + step, n_tp)), device_id_type=MESH
        )

    later_than[...] = jnp.where(
        lax.broadcasted_iota(jnp.int32, (span, span), 0)
        > lax.broadcasted_iota(jnp.int32, (span, span), 1),
        1.0,
        0.0,
    ).astype(jnp.bfloat16)

    load_gain.wait()
    load_query.start()
    load_value.start()
    gain = gain_in[...]
    step_rows = 16 if rows % 16 == 0 else rows

    def scale_rows(c):
        for first in range(starts[c], starts[c] + rows, step_rows):
            scaled[first : first + step_rows, :] = (
                x_in[first : first + step_rows, :].astype(jnp.float32) * gain
            ).astype(jnp.bfloat16)

    def project(c, weight):
        return jnp.dot(
            scaled[starts[c] : starts[c] + rows, :],
            weight[...],
            preferred_element_type=jnp.float32,
        )

    def factor_of(c):
        return jnp.concatenate(
            [
                inverse_rms(x_in[first : first + step_rows, :].astype(jnp.float32))
                for first in range(starts[c], starts[c] + rows, step_rows)
            ],
            axis=0,
        )

    def partner(order):
        return order + jnp.where(order >= me, 1, 0)

    def block_copy(part, order):
        to = partner(order)
        return pltpu.make_async_remote_copy(
            src_ref=outgoing.at[part * n_sp + to], dst_ref=landed.at[part * n_sp + me],
            send_sem=b_ssem, recv_sem=b_rsem,
            device_id=(to, lane), device_id_type=MESH,
        )

    def greet():
        pl.semaphore_wait(barrier, n_sp + n_tp - 2)

        @pl.loop(1, n_tp)
        def _(step):
            pl.semaphore_signal(
                ready, inc=1, device_id=(me, lax.rem(lane + step, n_tp)), device_id_type=MESH
            )

    for load in x_loads:
        load.wait()
    load_key.wait()
    wide_keys = []
    for c in range(chunks):
        scale_rows(c)
        wide_keys.append(project(c, wk))
    factor = jnp.concatenate([factor_of(c) for c in range(chunks)], axis=0)
    wide_keys = jnp.concatenate(wide_keys, axis=0) * factor
    inverse[...] = jnp.broadcast_to(factor, inverse.shape)
    keys[...] = wide_keys.astype(jnp.bfloat16)
    pack_blocks(wide_keys, outgoing, 0, heads, sub)

    @pl.when(upper == 1)
    def _():
        greet()
        block_copy(0, 0).start()

    load_next.wait()
    load_offset.wait()
    load_query.wait()
    load_value.wait()
    next_row = next_in[...].astype(jnp.float32)
    next_row = jnp.concatenate([next_row[n : n + 1] for n in range(next_row.shape[0])], axis=1)
    next_scaled = jnp.broadcast_to((next_row * gain).astype(jnp.bfloat16), (16, x_hbm.shape[1]))
    query = jnp.dot(next_scaled, wq[...], preferred_element_type=jnp.float32)
    query = query * inverse_rms(next_row)
    row_ids = lax.broadcasted_iota(jnp.int32, query.shape, 0)
    head_ids = lax.broadcasted_iota(jnp.int32, query.shape, 1) // HEAD_DIM
    query = jnp.where(row_ids == head_ids, query, 0.0).astype(jnp.bfloat16)
    wide_values = []
    for c in range(0):
        wide_values.append(project(c, wv))

    logits = lax.dot_general(
        query, keys[...], (((1,), (1,)), ((), ())), preferred_element_type=jnp.float32
    )[:heads]
    for c in range(0, chunks):
        wide_values.append(project(c, wv))
    logits = logits * HEAD_DIM ** (-0.5) + offset[...]
    tail = jnp.log1p(jnp.exp(-jnp.abs(logits)))
    log_breaks = -jnp.maximum(logits, 0.0) - tail
    inner = fold_parts(
        jnp.dot(split_parts(log_breaks, 3), later_than[...], preferred_element_type=jnp.float32),
        heads,
    )
    block_total = jnp.sum(log_breaks, axis=1, keepdims=True)
    weights = jnp.exp(jnp.minimum(logits, 0.0) - tail + inner)
    scale = inverse[...]
    wide_values = jnp.concatenate(wide_values, axis=0) * jnp.concatenate([scale] * heads, axis=1)
    read = fold_parts(
        jnp.dot(
            split_parts(weights, 2),
            wide_values.astype(jnp.bfloat16),
            preferred_element_type=jnp.float32,
        ),
        heads,
    )
    high = block_total.astype(jnp.bfloat16).astype(jnp.float32)
    low = block_total - high
    half = lax.broadcasted_iota(jnp.int32, (heads, HEAD_DIM), 1) < HEAD_DIM // 2
    message[...] = jnp.concatenate(
        [
            read[head : head + 1, head * HEAD_DIM : (head + 1) * HEAD_DIM]
            for head in range(heads)
        ]
        + [jnp.where(half, high, low)],
        axis=0,
    ).astype(jnp.bfloat16)
    gathered[me * n_tp + lane] = message[...]
    pack_blocks(wide_values, outgoing, n_sp, heads, sub)

    @pl.when(upper == 0)
    def _():
        greet()
        for order in range(early):
            block_copy(0, order).start()
            block_copy(1, order).start()

    pl.semaphore_wait(ready, n_tp - 1)

    def message_copy(to, step):
        return pltpu.make_async_remote_copy(
            src_ref=message, dst_ref=gathered.at[me * n_tp + lane],
            send_sem=m_ssem, recv_sem=m_rsem,
            device_id=(to, lax.rem(lane + step, n_tp)), device_id_type=MESH,
        )

    @pl.loop(0, n_sp - 1, unroll=unroll)
    def _(order):
        for step in range(n_tp):
            message_copy(partner(order), step).start()

    for step in range(1, n_tp):
        message_copy(me, step).start()

    @pl.when(upper == 1)
    def _():
        block_copy(1, 0).start()
        for order in range(1, early):
            block_copy(0, order).start()
            block_copy(1, order).start()

    @pl.loop(early, n_sp - 1, unroll=unroll)
    def _(order):
        block_copy(0, order).start()
        block_copy(1, order).start()

    landed[me] = outgoing[me]
    landed[n_sp + me] = outgoing[n_sp + me]

    everyone = gathered.at[pl.ds(0, n_sp * n_tp - 1)]
    pltpu.make_async_copy(everyone, everyone, m_rsem).wait()

    def add_block(step, carry):
        block = [gathered[(n_sp - 1 - step) * n_tp + part].astype(jnp.float32) for part in range(n_tp)]
        fresh = []
        for (total, carried), piece in zip(carry, block):
            total = total + jnp.exp(carried) * piece[:heads]
            halves = piece[heads:]
            fresh.append((total, carried + halves + pltpu.roll(halves, HEAD_DIM // 2, 1)))
        return tuple(fresh)

    zero = jnp.zeros((heads, HEAD_DIM), jnp.float32)
    totals = lax.fori_loop(0, n_sp, add_block, ((zero, zero),) * n_tp, unroll=unroll)
    read_out[...] = jnp.concatenate([total for total, _ in totals], axis=0).astype(jnp.bfloat16)

    pltpu.make_async_copy(everyone, everyone, m_ssem).wait()
    others = landed.at[pl.ds(0, 2 * n_sp - 2)]
    pltpu.make_async_copy(others, others, b_ssem).wait()
    pltpu.make_async_copy(others, others, b_rsem).wait()


def finish(landed, read_in, k_out, v_out, read_out):
    sub, n_sp, width = k_out.shape
    heads = width // HEAD_DIM
    for part, out in enumerate((k_out, v_out)):
        for head in range(heads):
            piece = landed[part * n_sp : (part + 1) * n_sp].astype(jnp.float32)[:, head * sub : (head + 1) * sub, :]
            out[:, :, head * HEAD_DIM : (head + 1) * HEAD_DIM] = jnp.swapaxes(
                piece, 0, 1
            ).astype(jnp.bfloat16)
    read_out[...] = read_in[...]


def shards(prompt_input, next_input, norm_gain, w_key, w_value, w_query, key_offset):
    span, depth = prompt_input.shape
    width = w_key.shape[1]
    heads = width // HEAD_DIM
    n_sp, n_tp = lax.axis_size("sp"), lax.axis_size("tp")
    sub = span // n_sp
    chunks = 2 if n_sp % 2 == 0 and span % 32 == 0 else 1
    wide, narrow = jnp.float32, jnp.bfloat16
    blocks = (2 * n_sp, heads * sub, HEAD_DIM)
    sems = pltpu.SemaphoreType.DMA
    landed = pl.pallas_call(
        functools.partial(kernel, n_sp, n_tp, chunks),
        out_shape=(
            jax.ShapeDtypeStruct(blocks, narrow),
            jax.ShapeDtypeStruct((n_tp * heads, HEAD_DIM), narrow),
        ),
        in_specs=[pl.BlockSpec(memory_space=pltpu.HBM)] * 7,
        out_specs=(pl.BlockSpec(memory_space=pltpu.VMEM),) * 2,
        scratch_shapes=[
            pltpu.VMEM((span, depth), narrow),
            pltpu.VMEM((span, depth), narrow),
            pltpu.VMEM((span, width), narrow),
            pltpu.VMEM((span, HEAD_DIM), wide),
            pltpu.VMEM((depth // HEAD_DIM, HEAD_DIM), narrow),
            pltpu.VMEM((1, depth), wide),
            pltpu.VMEM((depth, width), narrow),
            pltpu.VMEM((depth, width), narrow),
            pltpu.VMEM((depth, width), narrow),
            pltpu.VMEM((heads, span), wide),
            pltpu.VMEM((span, span), narrow),
            pltpu.VMEM(blocks, narrow),
            pltpu.VMEM((2 * heads, HEAD_DIM), narrow),
            pltpu.VMEM((n_sp * n_tp, 2 * heads, HEAD_DIM), narrow),
            sems((chunks,)),
            sems((6,)),
            sems,
            sems,
            sems,
            sems,
            pltpu.SemaphoreType.REGULAR,
        ],
        compiler_params=pltpu.CompilerParams(
            collective_id=0, has_side_effects=True, vmem_limit_bytes=16 * 2**20
        ),
        name="prefill",
    )(
        *[
            pltpu.with_memory_space_constraint(operand, pltpu.HBM)
            for operand in (
                prompt_input,
                next_input.reshape(-1, HEAD_DIM),
                norm_gain[None],
                w_key,
                w_value,
                w_query,
                key_offset.T,
            )
        ]
    )
    slotted = jax.ShapeDtypeStruct((sub, n_sp, width), narrow)
    key_cache, value_cache, reading = pl.pallas_call(
        finish,
        out_shape=(slotted, slotted, jax.ShapeDtypeStruct((n_tp * heads, HEAD_DIM), narrow)),
        in_specs=[pl.BlockSpec(memory_space=pltpu.VMEM)] * 2,
        out_specs=(pl.BlockSpec(memory_space=pltpu.VMEM),) * 3,
        compiler_params=pltpu.CompilerParams(vmem_limit_bytes=16 * 2**20),
        name="finish",
    )(*landed)
    return (
        jnp.swapaxes(key_cache, 0, 1)[None],
        jnp.swapaxes(value_cache, 0, 1)[None],
        reading.reshape(-1),
    )


def solution(mesh):
    placed = (P("sp", None), P(), P(), P(None, "tp"), P(None, "tp"), P(None, "tp"), P("sp", "tp"))
    return jax.shard_map(
        shards,
        mesh=mesh,
        in_specs=placed,
        out_specs=(P("sp", None, None, "tp"), P("sp", None, None, "tp"), P()),
        check_vma=False,
    )
```

time: 18.5 us -> 15.7 us (0.85)
  the two profiles are of different devices: /device:TPU:0 before, /device:TPU:24 now
where the time goes in v2:
time: 15.7 us; the launch traced here: 15.5 us
  Pallas kernels  14.8 us (94%)
  between operations  0.64 us (4%)
    pallas_call x1, Pallas kernels, shards(): pl.pallas_call(functools.partial(kernel, n_sp, n_tp, chunks), out_shape=(...  14 us
    pallas_call x1, Pallas kernels, shards(): pl.pallas_call(finish, out_shape=(slotted, slotted, jax.ShapeDtypeStruct(...  0.83 us

profile of v2, /device:TPU:24, one launch (start us, length us, event | category | flops | bytes accessed | tf_op | source)
XLA Modules:
  0.0 15.5 jit_solution(9749755161796520652)
XLA Ops:
  0.6 14.0 %prefill.1 = (bf16[16,72,128]{2,1,0:T(8,128)(2,1)S(1)}, bf16[8,128]{1,0:T(8,128)(2,1)S(1)}) custom-call(bf16[288,2048]{1,0:T(8,128)(2,1)} %x_hbm.1, bf16[16,128]{1,0:T(8,128)(2,1)} %bitcast.11, f32[1,2048]{1,0:T(1,128)} %bitcast.10, bf16[2048,256]{1,0:T(8,128)(2,1)} %wk_hbm.1, bf16[2048,256]{1,0:T(8,128)(2,1)} %wv_hbm.1, bf16[2048,256]{1,0:T(8,128)(2,1)} %wq_hbm.1, ...), custom_call_target="tpu_custom_call" | custom-call | tf_op jit(solution)/shard_map/prefill/pallas_call | solution.py:316
  14.6 0.8 %finish.1 = (bf16[36,8,256]{2,1,0:T(8,128)(2,1)}, bf16[36,8,256]{2,1,0:T(8,128)(2,1)}, bf16[8,128]{1,0:T(8,128)(2,1)}) custom-call(bf16[16,72,128]{2,1,0:T(8,128)(2,1)S(1)} %get-tuple-element.8.landed, bf16[8,128]{1,0:T(8,128)(2,1)S(1)} %get-tuple-element.9.read_in), custom_call_target="tpu_custom_call" | custom-call | tf_op jit(solution)/shard_map/finish/pallas_call | solution.py:366

commit v3 on v2

--- a/solution.py
+++ b/solution.py
@@ -60,7 +60,7 @@
     unroll = n_sp <= 16
 
     upper = me // ((n_sp + 1) // 2)
-    early = min(2, n_sp - 1)
+    early = min(4, n_sp - 1)
 
     load_gain, load_next, load_offset, load_key, load_query, load_value = [
         pltpu.make_async_copy(hbm, vmem, load_sem.at[n])
@@ -103,6 +103,8 @@
             barrier, inc=1, device_id=(me, lax.rem(lane + step, n_tp)), device_id_type=MESH
         )
 
+    load_query.start()
+    load_value.start()
     later_than[...] = jnp.where(
         lax.broadcasted_iota(jnp.int32, (span, span), 0)
         > lax.broadcasted_iota(jnp.int32, (span, span), 1),
@@ -111,35 +113,41 @@
     ).astype(jnp.bfloat16)
 
     load_gain.wait()
-    load_query.start()
-    load_value.start()
     gain = gain_in[...]
     step_rows = 16 if rows % 16 == 0 else rows
 
-    def scale_rows(c):
-        for first in range(starts[c], starts[c] + rows, step_rows):
-            scaled[first : first + step_rows, :] = (
-                x_in[first : first + step_rows, :].astype(jnp.float32) * gain
-            ).astype(jnp.bfloat16)
-
-    def project(c, weight):
-        return jnp.dot(
-            scaled[starts[c] : starts[c] + rows, :],
-            weight[...],
-            preferred_element_type=jnp.float32,
-        )
-
-    def factor_of(c):
-        return jnp.concatenate(
-            [
-                inverse_rms(x_in[first : first + step_rows, :].astype(jnp.float32))
-                for first in range(starts[c], starts[c] + rows, step_rows)
-            ],
-            axis=0,
+    depth = x_hbm.shape[1]
+    cut = depth // 2 if depth % 512 == 0 else depth
+
+    def norm_rows(c):
+        for first in range(c * rows, (c + 1) * rows, step_rows):
+            wide = x_in[first : first + step_rows, :].astype(jnp.float32)
+            scaled[first : first + step_rows, :] = (wide * gain).astype(jnp.bfloat16)
+            squares = wide * wide
+            inverse[first : first + step_rows, :] = sum(
+                squares[:, lane_group : lane_group + HEAD_DIM]
+                for lane_group in range(0, depth, HEAD_DIM)
+            )
+
+    def project(rows_in, weight, factor):
+        return sum(
+            jnp.dot(
+                rows_in[:, first : first + cut],
+                weight[first : first + cut, :],
+                preferred_element_type=jnp.float32,
+            )
+            * factor
+            for first in range(0, depth, cut)
         )
 
     def partner(order):
-        return order + jnp.where(order >= me, 1, 0)
+        falling = me - order
+        falling = falling + jnp.where(falling <= 0, n_sp - 1, 0)
+        falling = jnp.where(order == 0, 0, falling)
+        ahead = me + order + jnp.where(me == 0, 1, 0)
+        ahead = ahead - jnp.where(ahead >= n_sp, n_sp - 1, 0)
+        ahead = jnp.where(order == 0, jnp.where(me == 0, 1, 0), ahead)
+        return jnp.where(upper == 1, falling, ahead)
 
     def block_copy(part, order):
         to = partner(order)
@@ -158,16 +166,13 @@
                 ready, inc=1, device_id=(me, lax.rem(lane + step, n_tp)), device_id_type=MESH
             )
 
-    for load in x_loads:
-        load.wait()
+    for c in range(chunks):
+        x_loads[c].wait()
+        norm_rows(c)
     load_key.wait()
-    wide_keys = []
-    for c in range(chunks):
-        scale_rows(c)
-        wide_keys.append(project(c, wk))
-    factor = jnp.concatenate([factor_of(c) for c in range(chunks)], axis=0)
-    wide_keys = jnp.concatenate(wide_keys, axis=0) * factor
+    factor = lax.rsqrt(jnp.sum(inverse[...], axis=1, keepdims=True) * (1.0 / depth) + 1e-06)
     inverse[...] = jnp.broadcast_to(factor, inverse.shape)
+    wide_keys = project(scaled[...], wk, factor)
     keys[...] = wide_keys.astype(jnp.bfloat16)
     pack_blocks(wide_keys, outgoing, 0, heads, sub)
 
@@ -175,6 +180,8 @@
     def _():
         greet()
         block_copy(0, 0).start()
+        if n_sp > 3:
+            block_copy(0, me - 1).start()
 
     load_next.wait()
     load_offset.wait()
@@ -183,20 +190,18 @@
     next_row = next_in[...].astype(jnp.float32)
     next_row = jnp.concatenate([next_row[n : n + 1] for n in range(next_row.shape[0])], axis=1)
     next_scaled = jnp.broadcast_to((next_row * gain).astype(jnp.bfloat16), (16, x_hbm.shape[1]))
-    query = jnp.dot(next_scaled, wq[...], preferred_element_type=jnp.float32)
-    query = query * inverse_rms(next_row)
+    query = project(next_scaled, wq, inverse_rms(next_row))
     row_ids = lax.broadcasted_iota(jnp.int32, query.shape, 0)
     head_ids = lax.broadcasted_iota(jnp.int32, query.shape, 1) // HEAD_DIM
     query = jnp.where(row_ids == head_ids, query, 0.0).astype(jnp.bfloat16)
-    wide_values = []
-    for c in range(0):
-        wide_values.append(project(c, wv))
-
+    middle = span // 2 if span % 32 == 0 else span
+    factor = jnp.concatenate([inverse[...]] * heads, axis=1)
+    wide_values = [project(scaled[:middle, :], wv, factor[:middle])]
     logits = lax.dot_general(
         query, keys[...], (((1,), (1,)), ((), ())), preferred_element_type=jnp.float32
     )[:heads]
-    for c in range(0, chunks):
-        wide_values.append(project(c, wv))
+    if middle < span:
+        wide_values.append(project(scaled[middle:, :], wv, factor[middle:]))
     logits = logits * HEAD_DIM ** (-0.5) + offset[...]
     tail = jnp.log1p(jnp.exp(-jnp.abs(logits)))
     log_breaks = -jnp.maximum(logits, 0.0) - tail
@@ -206,8 +211,7 @@
     )
     block_total = jnp.sum(log_breaks, axis=1, keepdims=True)
     weights = jnp.exp(jnp.minimum(logits, 0.0) - tail + inner)
-    scale = inverse[...]
-    wide_values = jnp.concatenate(wide_values, axis=0) * jnp.concatenate([scale] * heads, axis=1)
+    wide_values = jnp.concatenate(wide_values, axis=0)
     read = fold_parts(
         jnp.dot(
             split_parts(weights, 2),
@@ -237,6 +241,10 @@
             block_copy(0, order).start()
             block_copy(1, order).start()
 
+    @pl.when(upper == 1)
+    def _():
+        block_copy(1, 0).start()
+
     pl.semaphore_wait(ready, n_tp - 1)
 
     def message_copy(to, step):
@@ -254,16 +262,14 @@
     for step in range(1, n_tp):
         message_copy(me, step).start()
 
-    @pl.when(upper == 1)
-    def _():
-        block_copy(1, 0).start()
-        for order in range(1, early):
+    sent = early * (1 - upper) + upper
+
+    @pl.loop(sent, n_sp - 1)
+    def _(order):
+        @pl.when((upper == 0) | (order != me - 1) | (n_sp <= 3))
+        def _():
             block_copy(0, order).start()
-            block_copy(1, order).start()
-
-    @pl.loop(early, n_sp - 1, unroll=unroll)
-    def _(order):
-        block_copy(0, order).start()
+
         block_copy(1, order).start()
 
     landed[me] = outgoing[me]
@@ -309,7 +315,7 @@
     heads = width // HEAD_DIM
     n_sp, n_tp = lax.axis_size("sp"), lax.axis_size("tp")
     sub = span // n_sp
-    chunks = 2 if n_sp % 2 == 0 and span % 32 == 0 else 1
+    chunks = 3 if span % 48 == 0 else 1
     wide, narrow = jnp.float32, jnp.bfloat16
     blocks = (2 * n_sp, heads * sub, HEAD_DIM)
     sems = pltpu.SemaphoreType.DMA

time: 15.7 us -> 14.9 us (0.949)
  the two profiles are of different devices: /device:TPU:24 before, /device:TPU:17 now
where the time goes in v3:
time: 14.9 us; the launch traced here: 14.6 us
  Pallas kernels  14 us (94%)
  between operations  0.64 us (4%)
    pallas_call x1, Pallas kernels, shards(): pl.pallas_call(functools.partial(kernel, n_sp, n_tp, chunks), out_shape=(...  13.2 us
    pallas_call x1, Pallas kernels, shards(): pl.pallas_call(finish, out_shape=(slotted, slotted, jax.ShapeDtypeStruct(...  0.83 us

profile of v3, /device:TPU:17, one launch (start us, length us, event | category | flops | bytes accessed | tf_op | source)
XLA Modules:
  0.0 14.6 jit_solution(11776364299969329097)
XLA Ops:
  0.6 13.2 %prefill.1 = (bf16[16,72,128]{2,1,0:T(8,128)(2,1)S(1)}, bf16[8,128]{1,0:T(8,128)(2,1)S(1)}) custom-call(bf16[288,2048]{1,0:T(8,128)(2,1)} %x_hbm.1, bf16[16,128]{1,0:T(8,128)(2,1)} %bitcast.11, f32[1,2048]{1,0:T(1,128)} %bitcast.10, bf16[2048,256]{1,0:T(8,128)(2,1)} %wk_hbm.1, bf16[2048,256]{1,0:T(8,128)(2,1)} %wv_hbm.1, bf16[2048,256]{1,0:T(8,128)(2,1)} %wq_hbm.1, ...), custom_call_target="tpu_custom_call" | custom-call | tf_op jit(solution)/shard_map/prefill/pallas_call | solution.py:322
  13.8 0.8 %finish.1 = (bf16[36,8,256]{2,1,0:T(8,128)(2,1)}, bf16[36,8,256]{2,1,0:T(8,128)(2,1)}, bf16[8,128]{1,0:T(8,128)(2,1)}) custom-call(bf16[16,72,128]{2,1,0:T(8,128)(2,1)S(1)} %get-tuple-element.8.landed, bf16[8,128]{1,0:T(8,128)(2,1)S(1)} %get-tuple-element.9.read_in), custom_call_target="tpu_custom_call" | custom-call | tf_op jit(solution)/shard_map/finish/pallas_call | solution.py:372

commit v4 on v3

--- a/solution.py
+++ b/solution.py
@@ -60,7 +60,7 @@
     unroll = n_sp <= 16
 
     upper = me // ((n_sp + 1) // 2)
-    early = min(4, n_sp - 1)
+    early = min(3, n_sp - 1)
 
     load_gain, load_next, load_offset, load_key, load_query, load_value = [
         pltpu.make_async_copy(hbm, vmem, load_sem.at[n])
@@ -144,6 +144,10 @@
         falling = me - order
         falling = falling + jnp.where(falling <= 0, n_sp - 1, 0)
         falling = jnp.where(order == 0, 0, falling)
+        second = me - order + 1
+        second = second + jnp.where(second <= 1, n_sp - 2, 0)
+        second = jnp.where(order <= 1, order, second)
+        falling = jnp.where(me >= n_sp - 2, falling, second)
         ahead = me + order + jnp.where(me == 0, 1, 0)
         ahead = ahead - jnp.where(ahead >= n_sp, n_sp - 1, 0)
         ahead = jnp.where(order == 0, jnp.where(me == 0, 1, 0), ahead)
@@ -181,7 +185,7 @@
         greet()
         block_copy(0, 0).start()
         if n_sp > 3:
-            block_copy(0, me - 1).start()
+            block_copy(0, jnp.where(me >= n_sp - 2, me - 1, 1)).start()
 
     load_next.wait()
     load_offset.wait()
@@ -237,7 +241,8 @@
     @pl.when(upper == 0)
     def _():
         greet()
-        for order in range(early):
+        block_copy(0, 0).start()
+        for order in range(1, early):
             block_copy(0, order).start()
             block_copy(1, order).start()
 
@@ -262,11 +267,15 @@
     for step in range(1, n_tp):
         message_copy(me, step).start()
 
+    @pl.when(upper == 0)
+    def _():
+        block_copy(1, 0).start()
+
     sent = early * (1 - upper) + upper
 
     @pl.loop(sent, n_sp - 1)
     def _(order):
-        @pl.when((upper == 0) | (order != me - 1) | (n_sp <= 3))
+        @pl.when((upper == 0) | (order != jnp.where(me >= n_sp - 2, me - 1, 1)) | (n_sp <= 3))
         def _():
             block_copy(0, order).start()
 

time: 14.9 us -> 14.7 us (0.987)
  the two profiles are of different devices: /device:TPU:17 before, /device:TPU:9 now
where the time goes in v4:
time: 14.7 us; the launch traced here: 14.5 us
  Pallas kernels  13.9 us (95%)
  between operations  0.64 us (4%)
    pallas_call x1, Pallas kernels, shards(): pl.pallas_call(functools.partial(kernel, n_sp, n_tp, chunks), out_shape=(...  13 us
    pallas_call x1, Pallas kernels, shards(): pl.pallas_call(finish, out_shape=(slotted, slotted, jax.ShapeDtypeStruct(...  0.83 us

profile of v4, /device:TPU:9, one launch (start us, length us, event | category | flops | bytes accessed | tf_op | source)
XLA Modules:
  0.0 14.5 jit_solution(1350987194808425997)
XLA Ops:
  0.6 13.0 %prefill.1 = (bf16[16,72,128]{2,1,0:T(8,128)(2,1)S(1)}, bf16[8,128]{1,0:T(8,128)(2,1)S(1)}) custom-call(bf16[288,2048]{1,0:T(8,128)(2,1)} %x_hbm.1, bf16[16,128]{1,0:T(8,128)(2,1)} %bitcast.11, f32[1,2048]{1,0:T(1,128)} %bitcast.10, bf16[2048,256]{1,0:T(8,128)(2,1)} %wk_hbm.1, bf16[2048,256]{1,0:T(8,128)(2,1)} %wv_hbm.1, bf16[2048,256]{1,0:T(8,128)(2,1)} %wq_hbm.1, ...), custom_call_target="tpu_custom_call" | custom-call | tf_op jit(solution)/shard_map/prefill/pallas_call | solution.py:331
  13.7 0.8 %finish.1 = (bf16[36,8,256]{2,1,0:T(8,128)(2,1)}, bf16[36,8,256]{2,1,0:T(8,128)(2,1)}, bf16[8,128]{1,0:T(8,128)(2,1)}) custom-call(bf16[16,72,128]{2,1,0:T(8,128)(2,1)S(1)} %get-tuple-element.8.landed, bf16[8,128]{1,0:T(8,128)(2,1)S(1)} %get-tuple-element.9.read_in), custom_call_target="tpu_custom_call" | custom-call | tf_op jit(solution)/shard_map/finish/pallas_call | solution.py:381
